TPU v7x, 32 devices: a whole 2x2x4 slice. The times are simulated.
32 devices in a mesh: grp: 2 (over x), ep: 8 (over z, y), tp: 2 (over core).
Axes of the slice: x: 2, y: 2, z: 4, core: 2. Of those that a mesh axis runs over, the one named last changes fastest.
Arguments:
- tokens: bfloat16 [4096, 2048], P(('grp', 'ep', 'tp')), parts along dimension 0, may hold values from -6 to 6
- norm_gain: float32 [2048], replicated, may hold values from 0.1 to 1.9
- expert_ids: int32 [4096, 2], P(('grp', 'ep', 'tp')), parts along dimension 0, may hold values from 0 to 7, all different within a row; in each aligned block of 128 rows (0 to 127, 128 to 255, ...) at most 64 rows name the same one
- route_weights: float32 [4096, 2], P(('grp', 'ep', 'tp')), parts along dimension 0, may hold values from 0.2 to 1
- gate_proj: bfloat16 [8, 2048, 1536], P('ep', None, 'tp'), may hold values from -0.375 to 0.375
- linear_proj: bfloat16 [8, 2048, 1536], P('ep', None, 'tp'), may hold values from -0.375 to 0.375
- down_proj: bfloat16 [8, 1536, 2048], P('ep', 'tp'), may hold values from -0.01953125 to 0.01953125
Outputs:
- mixed: bfloat16 [4096, 2048], P(('grp', 'ep', 'tp')), parts along dimension 0
There are 2 independent parts, one for each index of `grp`. A program takes and returns all parts, laid end to end along the dimension named above; an argument that names none is the same for every part. Nothing has to cross between parts.
Inputs may be any that keep to these rules, and one draw needn't show every extreme that they name: `expert_ids`: each token names 2 different experts. Among the 128 rows of one device (aligned blocks) no expert is named more than 64 times, a bound that some expert reaches in some blocks.
All inputs are finite; a program needn't handle non-finite values.
Results may differ from a plain program's by a relative error of at most 0.009.
Values may be sent and summed in bfloat16 or wider, within the bound.
A program may use at most 64 MiB of HBM per device.

v0:
```python
import functools

import jax
import jax.numpy as jnp
from jax import lax
from jax.experimental import pallas as pl
from jax.experimental.pallas import tpu as pltpu
from jax.sharding import PartitionSpec as P

MESH = pl.DeviceIdType.MESH
PARTS = 2


def shards(tokens, norm_gain, expert_ids, route_weights, gate_proj, linear_proj, down_proj):
    tok_count, width = tokens.shape
    picks = expert_ids.shape[1]
    experts = lax.axis_size("ep")
    capacity = 2 * tok_count * picks // experts
    values = tokens.astype(jnp.float32)
    normed = (
        values * lax.rsqrt(jnp.mean(values * values, axis=-1, keepdims=True) + 1e-06) * norm_gain
    ).astype(jnp.bfloat16)
    flat = expert_ids.reshape(-1)
    onehot = (flat[:, None] == jnp.arange(experts, dtype=jnp.int32)[None, :]).astype(jnp.int32)
    slots = jnp.sum((jnp.cumsum(onehot, axis=0) - 1) * onehot, axis=1)
    where = flat * capacity + slots
    buffer = (
        jnp.zeros((experts * capacity, width), jnp.bfloat16)
        .at[where]
        .set(jnp.repeat(normed, picks, axis=0))
    )
    arrived = lax.all_to_all(buffer, "ep", split_axis=0, concat_axis=0, tiled=True)
    rows = lax.all_gather(arrived, "tp", axis=0, tiled=True)
    gate_pre = jnp.dot(rows, gate_proj[0], preferred_element_type=jnp.float32)
    lin_pre = jnp.dot(rows, linear_proj[0], preferred_element_type=jnp.float32)
    glu = jnp.minimum(gate_pre, 7.0)
    lin = jnp.clip(lin_pre, -7.0, 7.0)
    hidden = (glu * jax.nn.sigmoid(1.702 * glu) * (lin + 1.0)).astype(jnp.bfloat16)
    rows = hidden
    summed = lax.psum_scatter(
        jnp.dot(rows, down_proj[0], preferred_element_type=jnp.float32).astype(jnp.bfloat16),
        "tp",
        scatter_dimension=0,
        tiled=True,
    )
    returned = lax.all_to_all(summed, "ep", split_axis=0, concat_axis=0, tiled=True)
    picked = returned[where].reshape(tok_count, picks, width).astype(jnp.float32)
    return jnp.sum(picked * route_weights[:, :, None], axis=1).astype(jnp.bfloat16)


def kernel(
    line, ids_ref, weights_ref, gain_ref, tokens_ref, gate_hbm, linear_hbm, down_hbm, out_ref,
    gate, linear, down, tok, meta, rows, cross, hidden, part, part_in, done, back_in, total,
    load_sem, tok_send, tok_recv, meta_send, meta_recv, cross_send, cross_recv, pair_send, pair_recv,
    part_send, part_recv, back_send, back_recv,
):
    ep, core = lax.axis_index("ep"), lax.axis_index("tp")
    z, y = ep // 2, ep % 2
    experts = 2 * line
    tok_count, width = tokens_ref.shape
    capacity = rows.shape[3]
    ff = gate.shape[1]
    half = width // PARTS
    cols = [slice(i * half, (i + 1) * half) for i in range(PARTS)]
    at_y = {"ep": z * 2 + 1 - y}
    at_core = {"tp": 1 - core}

    def at_z(other):
        return {"ep": other * 2 + y}

    def remote(source, target, send, recv, device):
        return pltpu.make_async_remote_copy(
            src_ref=source, dst_ref=target, send_sem=send, recv_sem=recv,
            device_id=device, device_id_type=MESH,
        )

    loads = [
        pltpu.make_async_copy(source, target, load_sem.at[i])
        for i, (source, target) in enumerate(((gate_hbm, gate), (linear_hbm, linear), (down_hbm, down)))
    ]
    for load in loads:
        load.start()
    barrier = pltpu.get_barrier_semaphore()
    for step in range(1, experts):
        pl.semaphore_signal(barrier, 1, device_id={"ep": (ep + step) % experts}, device_id_type=MESH)
    pl.semaphore_signal(barrier, 1, device_id=at_core, device_id_type=MESH)

    def normalize(i, _):
        span = pl.ds(pl.multiple_of(i * 32, 32), 32)
        values = tokens_ref[span, :].astype(jnp.float32)
        scale = lax.rsqrt(jnp.mean(values * values, axis=-1, keepdims=True) + 1e-06)
        tok[z, span, :] = (values * scale * gain_ref[...]).astype(jnp.bfloat16)
        return 0

    lax.fori_loop(0, tok_count // 32, normalize, 0)
    names = lax.broadcasted_iota(jnp.int32, (experts, tok_count), 0)
    share = jnp.zeros((experts, tok_count), jnp.float32)
    chosen = jnp.zeros((experts, tok_count), jnp.float32)
    for pick in range(ids_ref.shape[0]):
        same = ids_ref[pick : pick + 1, :] == names
        share = share + jnp.where(same, weights_ref[pick : pick + 1, :], 0.0)
        chosen = chosen + jnp.where(same, 1.0, 0.0)
    first = lax.broadcasted_iota(jnp.int32, (tok_count, tok_count), 0)
    second = lax.broadcasted_iota(jnp.int32, (tok_count, tok_count), 1)
    eye = first == second
    before = jnp.where(first < second, 1.0, 0.0).astype(jnp.bfloat16)
    slots = jnp.dot(chosen.astype(jnp.bfloat16), before, preferred_element_type=jnp.float32)
    meta[z, 0:experts, :] = jnp.where(chosen > 0.5, slots, -1.0)
    meta[z, experts : 2 * experts, :] = share
    pl.semaphore_wait(barrier, experts)

    def meta_copy(step):
        return remote(meta.at[z], meta.at[z], meta_send.at[step], meta_recv.at[z], at_z((z + step) % line))

    def meta_arrival(source):
        return remote(meta.at[source], meta.at[source], meta_send.at[0], meta_recv.at[source], at_z((z + 1) % line))

    for step in range(1, line):
        meta_copy(step).start()

    def order(step):
        found = z
        for place in range(line):
            nearest = sorted(range(line), key=lambda other: (abs(other - place), other))
            found = jnp.where(z == place, nearest[step], found)
        return found if step else z

    def hop(source, i, side):
        block = tok.at[source, :, cols[i]]
        return remote(
            block, block, tok_send.at[source, i, side], tok_recv.at[source, i],
            at_z(lax.rem(z + (1 if side else line - 1), line)),
        )

    def hops(source, i, act):
        @pl.when((source <= z) & (z < line - 1))
        def _():
            act(hop(source, i, 1))

        @pl.when((source >= z) & (z > 0))
        def _():
            act(hop(source, i, 0))

    def cross_copy(source, i):
        return remote(
            cross.at[source, :, cols[i]], rows.at[source, core, y, :, cols[i]],
            cross_send.at[source, i], cross_recv.at[source, i], at_y,
        )

    def cross_arrival(source, i):
        return remote(
            cross.at[source, :, cols[i]], rows.at[source, core, 1 - y, :, cols[i]],
            cross_send.at[source, i], cross_recv.at[source, i], at_y,
        )

    def pair_move(source, owner, column, i):
        block = rows.at[source, owner, column, :, cols[i]]
        return remote(block, block, pair_send.at[source, column, i], pair_recv.at[source, column, i], at_core)

    def part_copy(source, i):
        return remote(
            part.at[source, 1 - core, :, :, cols[i]], part_in.at[source, :, :, cols[i]],
            part_send.at[source, i], part_recv.at[source, i], at_core,
        )

    def back_copy(source, column, i):
        return remote(
            done.at[source, column, :, cols[i]], back_in.at[z, y, :, cols[i]],
            back_send.at[source, column, i], back_recv.at[z, y, i], {"ep": source * 2 + column},
        )

    def back_arrival(source, column, i):
        return remote(
            done.at[source, column, :, cols[i]], back_in.at[source, column, :, cols[i]],
            back_send.at[source, column, i], back_recv.at[source, column, i], {"ep": source * 2 + column},
        )

    tile = 512

    def over_width(i, act):
        def go(j, _):
            act(pl.ds(pl.multiple_of(i * half + j * tile, tile), tile))
            return 0

        lax.fori_loop(0, half // tile, go, 0)

    def arrive(tick, i):
        if tick == 0:
            hops(z, i, lambda copy: copy.start())
        for step in range(max(tick, 1), line):
            source = order(step)
            apart = jnp.where(source > z, source - z, z - source)

            @pl.when(apart == tick)
            def _():
                hop(source, i, 0).wait_recv()
                hops(source, i, lambda copy: copy.start())

    def dispatch(step):
        source = order(step)
        place = lax.broadcasted_iota(jnp.int32, (capacity, tok_count), 0).astype(jnp.float32)
        if step:
            meta_arrival(source).wait_recv()
        away = (meta[source, pl.ds(z * 2 + 1 - y, 1), :] == place).astype(jnp.bfloat16)
        here = (meta[source, pl.ds(z * 2 + y, 1), :] == place).astype(jnp.bfloat16)

        def send_away(span):
            cross[source, :, span] = jnp.dot(
                away, tok[source, :, span], preferred_element_type=jnp.float32
            ).astype(jnp.bfloat16)

        def keep_here(span):
            rows[source, core, y, :, span] = jnp.dot(
                here, tok[source, :, span], preferred_element_type=jnp.float32
            ).astype(jnp.bfloat16)

        if step == 0:
            for i in range(PARTS):
                arrive(step, i)
        for i in range(PARTS):
            if step:
                arrive(step, i)
            over_width(i, send_away)
            cross_copy(source, i).start()
            over_width(i, keep_here)
            pair_move(source, core, y, i).start()

    def forward(step):
        source = order(step)
        for i in range(PARTS):
            cross_arrival(source, i).wait_recv()
            pair_move(source, core, 1 - y, i).start()

    def compute(step):
        source = order(step)
        for column in range(2):
            for i in range(PARTS):
                pair_move(source, 1 - core, column, i).wait_recv()
        if step == 0:
            loads[0].wait()
            loads[1].wait()
        depth = 256

        def up(i, _):
            span = pl.ds(pl.multiple_of(i * depth, depth), depth)
            block = rows[source].reshape(4 * capacity, width)
            glu = jnp.minimum(jnp.dot(block, gate[:, span], preferred_element_type=jnp.float32), 7.0)
            lin = jnp.clip(jnp.dot(block, linear[:, span], preferred_element_type=jnp.float32), -7.0, 7.0)
            hidden[:, span] = (glu * jax.nn.sigmoid(1.702 * glu) * (lin + 1.0)).astype(jnp.bfloat16)
            return 0

        lax.fori_loop(0, ff // depth, up, 0)
        if step == 0:
            loads[2].wait()

        def out(span):
            part[source, :, :, :, span] = (
                jnp.dot(hidden[...], down[:, span], preferred_element_type=jnp.float32)
                .astype(jnp.bfloat16)
                .reshape(2, 2, capacity, tile)
            )

        for i in range(PARTS):
            over_width(i, out)
            part_copy(source, i).start()

    def finish(step):
        source = order(step)

        def add(span):
            whole = part[source, core, :, :, span].astype(jnp.float32) + part_in[source, :, :, span].astype(
                jnp.float32
            )
            done[source, :, :, span] = whole.astype(jnp.bfloat16)

        for i in range(PARTS):
            part_copy(source, i).wait_recv()
            over_width(i, add)
            back_copy(source, 1 - y, i).start()
            if step:
                back_copy(source, y, i).start()

    def gather(step, other):
        source, column = order(step), 1 - y if other else y
        expert = source * 2 + column
        lane = lax.broadcasted_iota(jnp.int32, (tok_count, capacity), 1).astype(jnp.float32)

        def upright(row):
            return jnp.sum(jnp.where(eye, meta[z, pl.ds(row, 1), :], 0.0), axis=1, keepdims=True)

        spread = (upright(expert) == lane).astype(jnp.bfloat16)
        share_here = upright(experts + expert)
        own = step == 0 and not other

        def merge(span):
            block = done[source, column, :, span] if own else back_in[source, column, :, span]
            term = share_here * jnp.dot(spread, block, preferred_element_type=jnp.float32)
            if own:
                total[:, span] = term
            elif step == line - 1 and other:
                out_ref[:, span] = (total[:, span] + term).astype(jnp.bfloat16)
            else:
                total[:, span] = total[:, span] + term

        for i in range(PARTS):
            if not own:
                back_arrival(source, column, i).wait_recv()
            over_width(i, merge)

    for tick in range(line + 1):
        if tick < line:
            dispatch(tick)
        if tick:
            compute(tick - 1)
            finish(tick - 1)
        if tick < line:
            forward(tick)
    for step in range(line):
        gather(step, False)
        gather(step, True)
    for step in range(line):
        source = order(step)
        if step:
            meta_copy(step).wait_send()
        for i in range(PARTS):
            hops(source, i, lambda copy: copy.wait_send())
            back_copy(source, 1 - y, i).wait_send()
            if step:
                back_copy(source, y, i).wait_send()
            cross_copy(source, i).wait_send()
            for column in range(2):
                pair_move(source, core, column, i).wait_send()
            part_copy(source, i).wait_send()


def fused(line, tokens, norm_gain, expert_ids, route_weights, gate_proj, linear_proj, down_proj):
    tok_count, width = tokens.shape
    picks = expert_ids.shape[1]
    experts = 2 * line
    capacity = 2 * tok_count * picks // experts
    ff = gate_proj.shape[2]
    wide, dma = jnp.bfloat16, pltpu.SemaphoreType.DMA
    inside, outside = pl.BlockSpec(memory_space=pltpu.VMEM), pl.BlockSpec(memory_space=pl.ANY)
    return pl.pallas_call(
        functools.partial(kernel, line),
        out_shape=jax.ShapeDtypeStruct((tok_count, width), wide),
        in_specs=[inside] * 4 + [outside] * 3,
        out_specs=inside,
        scratch_shapes=[
            pltpu.VMEM((width, ff), wide),
            pltpu.VMEM((width, ff), wide),
            pltpu.VMEM((ff, width), wide),
            pltpu.VMEM((line, tok_count, width), wide),
            pltpu.VMEM((line, 2 * experts, tok_count), jnp.float32),
            pltpu.VMEM((line, 2, 2, capacity, width), wide),
            pltpu.VMEM((line, capacity, width), wide),
            pltpu.VMEM((4 * capacity, ff), wide),
            pltpu.VMEM((line, 2, 2, capacity, width), wide),
            pltpu.VMEM((line, 2, capacity, width), wide),
            pltpu.VMEM((line, 2, capacity, width), wide),
            pltpu.VMEM((line, 2, capacity, width), wide),
            pltpu.VMEM((tok_count, width), jnp.float32),
            dma((3,)),
            dma((line, PARTS, 2)), dma((line, PARTS)),
            dma((line,)), dma((line,)),
            dma((line, PARTS)), dma((line, PARTS)),
            dma((line, 2, PARTS)), dma((line, 2, PARTS)),
            dma((line, PARTS)), dma((line, PARTS)),
            dma((line, 2, PARTS)), dma((line, 2, PARTS)),
        ],
        compiler_params=pltpu.CompilerParams(
            collective_id=0, has_side_effects=True, vmem_limit_bytes=60 * 1024 * 1024
        ),
        name="experts",
    )(
        expert_ids.T, route_weights.T, norm_gain.reshape(1, width), tokens,
        gate_proj[0], linear_proj[0], down_proj[0],
    )


def solution(mesh):
    placed = (
        P(("grp", "ep", "tp"), None),
        P(),
        P(("grp", "ep", "tp"), None),
        P(("grp", "ep", "tp"), None),
        P("ep", None, "tp"),
        P("ep", None, "tp"),
        P("ep", "tp", None),
    )
    along = [device.coords[2] for device in mesh.devices[0, :, 0]]
    line = len(set(along))
    paired = line > 1 and along == [index // 2 for index in range(2 * line)] and mesh.shape["tp"] == 2
    return jax.shard_map(
        functools.partial(fused, line) if paired else shards,
        mesh=mesh,
        in_specs=placed,
        out_specs=P(("grp", "ep", "tp"), None),
        check_vma=False,
    )
```

profile of v0, /device:TPU:24, one launch (start us, length us, event | category | flops | bytes accessed | tf_op | source)
XLA Modules:
  0.0 96.1 jit_solution(6821109383793381782)
XLA Ops:
  0.0 94.3 %experts.1 = bf16[128,2048]{1,0:T(8,128)(2,1)} custom-call(s32[2,128]{1,0:T(2,128)} %bitcast.10, f32[2,128]{1,0:T(2,128)} %bitcast.11, f32[1,2048]{1,0:T(1,128)} %bitcast.9, bf16[128,2048]{1,0:T(8,128)(2,1)} %tokens_ref.1, bf16[2048,768]{1,0:T(8,128)(2,1)} %bitcast.6, bf16[2048,768]{1,0:T(8,128)(2,1)} %bitcast.7, bf16[768,2048]{1,0:T(8,128)(2,1)} %bitcast.8), custom_call_target="tpu_custom_call" | custom-call | tf_op jit(solution)/shard_map/experts/pallas_call | solution.py:344
  94.3 1.9 %copy.9 = bf16[128,2048]{1,0:T(8,128)(2,1)} copy(bf16[128,2048]{1,0:T(8,128)(2,1)} %experts.1) | data formatting | bytes 1048576
where the time goes:
time: 96.3 us; the launch traced here: 96.1 us
  Pallas kernels  94.3 us (98%)
  local copies, waits for them, and re-layouts  1.88 us (2%)
    pallas_call x1, Pallas kernels, fused(): pl.pallas_call(functools.partial(kernel, line), out_shape=jax.ShapeDtypeS...  94.3 us

commit v1 on v0

v1 whole, which is shorter than its diff:
```python
import functools

import jax
import jax.numpy as jnp
from jax import lax
from jax.experimental import pallas as pl
from jax.experimental.pallas import tpu as pltpu
from jax.sharding import PartitionSpec as P

MESH = pl.DeviceIdType.MESH
LINE = 4
PARTS = 8
BANDS = 4
EARLY = 1

OUTER_PLAN = (
    0, 1, 2, 3, 4, 5, 6, 7, 500, 100, 10, 101, 510, 102, 11, 103, 104, 12, 105, 106,
    13, 107, 110, 200, 14, 111, 112, 201, 15, 113, 202, 300, 16, 114, 301, 302, 17, 115, 400, 303,
    401, 402, 30, 530, 116, 403, 117, 20, 520, 210, 21, 211, 212, 22, 120, 310, 311, 23, 121, 312,
    313, 24, 130, 410, 411, 122, 412, 413, 25, 123, 124, 26, 610, 611, 27, 612, 613, 31, 614, 615,
    32, 616, 617, 33, 125, 126, 34, 127, 131, 35, 220, 221, 36, 222, 37, 320, 321, 322, 323, 420,
    132, 133, 134, 135, 136, 421, 137, 422, 423, 800, 801, 802, 803, 804, 805, 806, 807, 230, 620, 231,
    621, 232, 622, 623, 330, 624, 331, 625, 332, 430, 626, 627, 431, 333, 432, 433, 600, 630, 601, 631,
    632, 602, 633, 634, 603, 635, 636, 604, 637, 605, 606, 607,
)
INNER_PLAN = (
    0, 1, 2, 3, 4, 5, 6, 7, 500, 100, 10, 510, 30, 530, 101, 102, 11, 103, 104, 12,
    105, 20, 520, 106, 13, 107, 21, 110, 200, 22, 130, 14, 111, 201, 23, 15, 112, 120, 202, 16,
    113, 300, 121, 301, 24, 17, 701, 702, 703, 704, 705, 706, 707, 122, 302, 114, 400, 303, 25, 123,
    401, 402, 115, 26, 403, 116, 124, 27, 117, 125, 31, 210, 126, 211, 127, 32, 212, 131, 33, 220,
    221, 222, 132, 133, 34, 35, 320, 321, 322, 36, 323, 420, 421, 134, 310, 37, 422, 135, 311, 423,
    800, 801, 802, 803, 804, 805, 806, 807, 312, 136, 313, 410, 411, 412, 413, 137, 230, 231, 232, 330,
    331, 332, 333, 430, 431, 432, 433, 620, 621, 622, 610, 623, 611, 624, 612, 625, 613, 626, 614, 627,
    615, 630, 616, 631, 617, 632, 600, 633, 601, 634, 602, 635, 603, 636, 604, 637, 605, 606, 607,
)


def shards(tokens, norm_gain, expert_ids, route_weights, gate_proj, linear_proj, down_proj):
    tok_count, width = tokens.shape
    picks = expert_ids.shape[1]
    experts = lax.axis_size("ep")
    capacity = 2 * tok_count * picks // experts
    values = tokens.astype(jnp.float32)
    normed = (
        values * lax.rsqrt(jnp.mean(values * values, axis=-1, keepdims=True) + 1e-06) * norm_gain
    ).astype(jnp.bfloat16)
    flat = expert_ids.reshape(-1)
    onehot = (flat[:, None] == jnp.arange(experts, dtype=jnp.int32)[None, :]).astype(jnp.int32)
    slots = jnp.sum((jnp.cumsum(onehot, axis=0) - 1) * onehot, axis=1)
    where = flat * capacity + slots
    buffer = (
        jnp.zeros((experts * capacity, width), jnp.bfloat16)
        .at[where]
        .set(jnp.repeat(normed, picks, axis=0))
    )
    arrived = lax.all_to_all(buffer, "ep", split_axis=0, concat_axis=0, tiled=True)
    rows = lax.all_gather(arrived, "tp", axis=0, tiled=True)
    gate_pre = jnp.dot(rows, gate_proj[0], preferred_element_type=jnp.float32)
    lin_pre = jnp.dot(rows, linear_proj[0], preferred_element_type=jnp.float32)
    glu = jnp.minimum(gate_pre, 7.0)
    lin = jnp.clip(lin_pre, -7.0, 7.0)
    hidden = (glu * jax.nn.sigmoid(1.702 * glu) * (lin + 1.0)).astype(jnp.bfloat16)
    rows = hidden
    summed = lax.psum_scatter(
        jnp.dot(rows, down_proj[0], preferred_element_type=jnp.float32).astype(jnp.bfloat16),
        "tp",
        scatter_dimension=0,
        tiled=True,
    )
    returned = lax.all_to_all(summed, "ep", split_axis=0, concat_axis=0, tiled=True)
    picked = returned[where].reshape(tok_count, picks, width).astype(jnp.float32)
    return jnp.sum(picked * route_weights[:, :, None], axis=1).astype(jnp.bfloat16)


def kernel(
    ids_ref, weights_ref, gain_ref, tokens_ref, gate_hbm, linear_hbm, down_hbm, out_ref,
    gate, linear, down, tok, meta, pick, spread, shares, rows, cross, hidden, part, part_in, done,
    back_in, ret_in, ret_out,
    load_sem, tok_send, tok_recv, meta_send, meta_recv, cross_send, cross_recv, pair_send, pair_recv,
    part_send, part_recv, back_send, back_recv, ret_send, ret_recv,
):
    ep, core = lax.axis_index("ep"), lax.axis_index("tp")
    z, y = ep // 2, ep % 2
    experts = 2 * LINE
    tok_count, width = tokens_ref.shape
    capacity = rows.shape[3]
    ff = gate.shape[1]
    cols = [pl.ds(i * (width // PARTS), width // PARTS) for i in range(PARTS)]
    bands = [pl.ds(i * (width // BANDS), width // BANDS) for i in range(BANDS)]
    units = [pl.ds(i * 256, 256) for i in range(ff // 256)]
    here, there = z * 2 + y, z * 2 + 1 - y
    at_y = {"ep": there}
    at_core = {"tp": 1 - core}
    outwards = jnp.where(z < LINE // 2, -1, 1)
    outer = (z == 0) | (z == LINE - 1)

    def at_z(other):
        return {"ep": other * 2 + y}

    def remote(source, target, send, recv, device):
        return pltpu.make_async_remote_copy(
            src_ref=source, dst_ref=target, send_sem=send, recv_sem=recv,
            device_id=device, device_id_type=MESH,
        )

    loads = [
        pltpu.make_async_copy(source, target, load_sem.at[i])
        for i, (source, target) in enumerate(((gate_hbm, gate), (linear_hbm, linear), (down_hbm, down)))
    ]
    for load in loads:
        load.start()
    barrier = pltpu.get_barrier_semaphore()
    for step in range(1, LINE):
        pl.semaphore_signal(barrier, 1, device_id=at_z(lax.rem(z + step, LINE)), device_id_type=MESH)
    pl.semaphore_signal(barrier, 1, device_id=at_y, device_id_type=MESH)
    pl.semaphore_signal(barrier, 1, device_id=at_core, device_id_type=MESH)

    def normalize(i, _):
        span = pl.ds(pl.multiple_of(i * 32, 32), 32)
        values = tokens_ref[span, :].astype(jnp.float32)
        scale = lax.rsqrt(jnp.mean(values * values, axis=-1, keepdims=True) + 1e-06)
        tok[z, span, :] = (values * scale * gain_ref[...]).astype(jnp.bfloat16)
        return 0

    lax.fori_loop(0, tok_count // 32, normalize, 0)
    names = lax.broadcasted_iota(jnp.int32, (experts, tok_count), 0)
    share = jnp.zeros((experts, tok_count), jnp.float32)
    chosen = jnp.zeros((experts, tok_count), jnp.float32)
    for choice in range(ids_ref.shape[0]):
        same = ids_ref[choice : choice + 1, :] == names
        share = share + jnp.where(same, weights_ref[choice : choice + 1, :], 0.0)
        chosen = chosen + jnp.where(same, 1.0, 0.0)
    first = lax.broadcasted_iota(jnp.int32, (tok_count, tok_count), 0)
    second = lax.broadcasted_iota(jnp.int32, (tok_count, tok_count), 1)
    before = jnp.where(first < second, 1.0, 0.0).astype(jnp.bfloat16)
    slots = jnp.dot(chosen.astype(jnp.bfloat16), before, preferred_element_type=jnp.float32)
    meta[z, 0:experts, :] = jnp.where(chosen > 0.5, slots, -1.0)
    meta[z, experts : 2 * experts, :] = share
    pl.semaphore_wait(barrier, LINE + 1)

    def meta_copy(step):
        return remote(
            meta.at[z], meta.at[z], meta_send.at[step], meta_recv.at[z], at_z(lax.rem(z + step, LINE))
        )

    def meta_arrival(source):
        return remote(
            meta.at[source], meta.at[source], meta_send.at[0], meta_recv.at[source],
            at_z(lax.rem(z + 1, LINE)),
        )

    def hop(source, i, way):
        block = tok.at[source, :, cols[i]]
        other = z + outwards if way else z - outwards
        return remote(
            block, block, tok_send.at[source, i, way], tok_recv.at[source, i], at_z(other)
        )

    def cross_copy(source, i):
        return remote(
            cross.at[source, :, cols[i]], rows.at[source, core, y, :, cols[i]],
            cross_send.at[source, i], cross_recv.at[source, i], at_y,
        )

    def cross_arrival(source, i):
        return remote(
            cross.at[source, :, cols[i]], rows.at[source, core, 1 - y, :, cols[i]],
            cross_send.at[source, i], cross_recv.at[source, i], at_y,
        )

    def pair_move(source, owner, column, i):
        block = rows.at[source, owner, column, :, cols[i]]
        return remote(block, block, pair_send.at[source, column, i], pair_recv.at[source, column, i], at_core)

    def part_copy(source, i):
        return remote(
            part.at[source, 1 - core, :, :, bands[i]], part_in.at[source, :, :, bands[i]],
            part_send.at[source, i], part_recv.at[source, i], at_core,
        )

    def back_copy(source, i):
        return remote(
            done.at[source, 1 - y, :, cols[i]], back_in.at[source, :, cols[i]],
            back_send.at[source, i], back_recv.at[source, i], at_y,
        )

    def ret_copy(source, i, way):
        step = outwards if way else -outwards
        side = jnp.where(step > 0, 0, 1)
        return remote(
            ret_out.at[source, :, cols[i]], ret_in.at[side, source, :, cols[i]],
            ret_send.at[source, i], ret_recv.at[side, source, i], at_z(z + step),
        )

    def ret_arrival(source, i, way):
        step = -outwards if way else outwards
        side = jnp.where(step > 0, 0, 1)
        return side, remote(
            ret_out.at[source, :, cols[i]], ret_in.at[side, source, :, cols[i]],
            ret_send.at[source, i], ret_recv.at[side, source, i], at_z(z - step),
        )

    def run(plan, at_end):
        if at_end:
            order = [z, z - outwards, z - 3 * outwards, z - 2 * outwards]
            passes = [(0,), (), (), ()]
            leaves = [None, 0, 0, 0]
            comes = [(0,), (), (), ()]
        else:
            order = [z, z + outwards, z - 2 * outwards, z - outwards]
            passes = [(1, 0), (0,), (1,), (1,)]
            leaves = [None, 1, 0, 0]
            comes = [(0, 1), (0,), (1,), (1,)]
        waited = [False, False]

        def send_rows(t, i):
            source = order[t]
            if t:
                hop(source, i, 0).wait_recv()
                for way in passes[t]:
                    hop(source, i, way).start()
            if i == 0:
                if t:
                    meta_arrival(source).wait_recv()
                place = lax.broadcasted_iota(jnp.int32, (capacity, tok_count), 0).astype(jnp.float32)
                for half, expert in enumerate((there, here)):
                    pick[t, half * capacity : (half + 1) * capacity, :] = (
                        meta[source, pl.ds(expert, 1), :] == place
                    ).astype(jnp.bfloat16)
            both = jnp.dot(
                pick[t], tok[source, :, cols[i]], preferred_element_type=jnp.float32
            ).astype(jnp.bfloat16)
            cross[source, :, cols[i]] = both[:capacity]
            cross_copy(source, i).start()
            rows[source, core, y, :, cols[i]] = both[capacity:]
            pair_move(source, core, y, i).start()

        def share_rows(t, i):
            source = order[t]
            cross_arrival(source, i).wait_recv()
            pair_move(source, core, 1 - y, i).start()

        def up(t, i):
            source = order[t]
            if i == 0:
                for column in range(2):
                    for j in range(PARTS):
                        pair_move(source, 1 - core, column, j).wait_recv()
                if not waited[0]:
                    waited[0] = True
                    loads[0].wait()
                    loads[1].wait()
            block = rows[source].reshape(4 * capacity, width)
            glu = jnp.minimum(jnp.dot(block, gate[:, units[i]], preferred_element_type=jnp.float32), 7.0)
            lin = jnp.clip(jnp.dot(block, linear[:, units[i]], preferred_element_type=jnp.float32), -7.0, 7.0)
            hidden[t, :, units[i]] = (glu * jax.nn.sigmoid(1.702 * glu) * (lin + 1.0)).astype(jnp.bfloat16)

        def out(t, i):
            source = order[t]
            if not waited[1]:
                waited[1] = True
                loads[2].wait()
            part[source, :, :, :, bands[i]] = (
                jnp.dot(hidden[t], down[:, bands[i]], preferred_element_type=jnp.float32)
                .astype(jnp.bfloat16)
                .reshape(2, 2, capacity, width // BANDS)
            )
            part_copy(source, i).start()

        def add(t, i):
            source = order[t]
            part_copy(source, i).wait_recv()
            done[source, :, :, bands[i]] = (
                part[source, core, :, :, bands[i]].astype(jnp.float32)
                + part_in[source, :, :, bands[i]].astype(jnp.float32)
            ).astype(jnp.bfloat16)
            if t:
                for j in range(i * PARTS // BANDS, (i + 1) * PARTS // BANDS):
                    back_copy(source, j).start()

        def turn(t, i):
            source = order[t]
            eye = lax.broadcasted_iota(jnp.int32, (tok_count, tok_count), 0) == lax.broadcasted_iota(
                jnp.int32, (tok_count, tok_count), 1
            )
            lane = lax.broadcasted_iota(jnp.int32, (tok_count, capacity), 1).astype(jnp.float32)

            def upright(row):
                return jnp.sum(jnp.where(eye, meta[source, pl.ds(row, 1), :], 0.0), axis=1, keepdims=True)

            for half, expert in enumerate((here, there)):
                spread[t, half] = (upright(expert) == lane).astype(jnp.bfloat16)
                shares[t, half] = jnp.broadcast_to(upright(experts + expert), (tok_count, 128))

        def merge(t, i):
            source = order[t]
            back_copy(source, i).wait_recv()
            total = None
            for half, block in enumerate((done[source, y, :, cols[i]], back_in[source, :, cols[i]])):
                scale = jnp.concatenate([shares[t, half]] * (width // PARTS // 128), axis=1)
                term = scale * jnp.dot(spread[t, half], block, preferred_element_type=jnp.float32)
                total = term if total is None else total + term
            for way in comes[t]:
                side, arrival = ret_arrival(source, i, way)
                arrival.wait_recv()
                total = total + ret_in[side, source, :, cols[i]].astype(jnp.float32)
            if t:
                ret_out[source, :, cols[i]] = total.astype(jnp.bfloat16)
                ret_copy(source, i, leaves[t]).start()
            else:
                out_ref[:, cols[i]] = total.astype(jnp.bfloat16)

        def late(t, i):
            hop(z, i, 0).start()

        def own_back(t, i):
            back_copy(z, i).start()

        for step in range(1, LINE):
            meta_copy(step).start()
        for way in passes[0]:
            for i in range(PARTS if at_end or way else EARLY):
                hop(z, i, way).start()
        stages = (send_rows, share_rows, up, out, add, turn, merge, late, own_back)
        for number in plan:
            stages[number // 100](number // 10 % 10, number % 10)
        for step in range(1, LINE):
            meta_copy(step).wait_send()
        for t in range(LINE):
            source = order[t]
            for i in range(PARTS):
                for way in passes[t]:
                    hop(source, i, way).wait_send()
                cross_copy(source, i).wait_send()
                for column in range(2):
                    pair_move(source, core, column, i).wait_send()
                back_copy(source, i).wait_send()
                if t:
                    ret_copy(source, i, leaves[t]).wait_send()
            for i in range(BANDS):
                part_copy(source, i).wait_send()

    pl.when(outer)(lambda: run(OUTER_PLAN, True))
    pl.when(jnp.logical_not(outer))(lambda: run(INNER_PLAN, False))


def fused(tokens, norm_gain, expert_ids, route_weights, gate_proj, linear_proj, down_proj):
    tok_count, width = tokens.shape
    picks = expert_ids.shape[1]
    experts = 2 * LINE
    capacity = 2 * tok_count * picks // experts
    ff = gate_proj.shape[2]
    wide, dma = jnp.bfloat16, pltpu.SemaphoreType.DMA
    inside, outside = pl.BlockSpec(memory_space=pltpu.VMEM), pl.BlockSpec(memory_space=pl.ANY)
    return pl.pallas_call(
        kernel,
        out_shape=jax.ShapeDtypeStruct((tok_count, width), wide),
        in_specs=[inside] * 4 + [outside] * 3,
        out_specs=inside,
        scratch_shapes=[
            pltpu.VMEM((width, ff), wide),
            pltpu.VMEM((width, ff), wide),
            pltpu.VMEM((ff, width), wide),
            pltpu.VMEM((LINE, tok_count, width), wide),
            pltpu.VMEM((LINE, 2 * experts, tok_count), jnp.float32),
            pltpu.VMEM((LINE, 2 * capacity, tok_count), wide),
            pltpu.VMEM((LINE, 2, tok_count, capacity), wide),
            pltpu.VMEM((LINE, 2, tok_count, 128), jnp.float32),
            pltpu.VMEM((LINE, 2, 2, capacity, width), wide),
            pltpu.VMEM((LINE, capacity, width), wide),
            pltpu.VMEM((LINE, 4 * capacity, ff), wide),
            pltpu.VMEM((LINE, 2, 2, capacity, width), wide),
            pltpu.VMEM((LINE, 2, capacity, width), wide),
            pltpu.VMEM((LINE, 2, capacity, width), wide),
            pltpu.VMEM((LINE, capacity, width), wide),
            pltpu.VMEM((2, LINE, tok_count, width), wide),
            pltpu.VMEM((LINE, tok_count, width), wide),
            dma((3,)),
            dma((LINE, PARTS, 2)), dma((LINE, PARTS)),
            dma((LINE,)), dma((LINE,)),
            dma((LINE, PARTS)), dma((LINE, PARTS)),
            dma((LINE, 2, PARTS)), dma((LINE, 2, PARTS)),
            dma((LINE, BANDS)), dma((LINE, BANDS)),
            dma((LINE, PARTS)), dma((LINE, PARTS)),
            dma((LINE, PARTS)), dma((2, LINE, PARTS)),
        ],
        compiler_params=pltpu.CompilerParams(
            collective_id=0, has_side_effects=True, vmem_limit_bytes=60 * 1024 * 1024
        ),
        name="experts",
    )(
        expert_ids.T, route_weights.T, norm_gain.reshape(1, width), tokens,
        gate_proj[0], linear_proj[0], down_proj[0],
    )


def solution(mesh):
    placed = (
        P(("grp", "ep", "tp"), None),
        P(),
        P(("grp", "ep", "tp"), None),
        P(("grp", "ep", "tp"), None),
        P("ep", None, "tp"),
        P("ep", None, "tp"),
        P("ep", "tp", None),
    )
    along = [device.coords[2] for device in mesh.devices[0, :, 0]]
    planned = along == [index // 2 for index in range(2 * LINE)] and mesh.shape["tp"] == 2
    return jax.shard_map(
        fused if planned else shards,
        mesh=mesh,
        in_specs=placed,
        out_specs=P(("grp", "ep", "tp"), None),
        check_vma=False,
    )
```

time: 96.3 us -> 81.9 us (0.85)
  the two profiles are of different devices: /device:TPU:24 before, /device:TPU:10 now
where the time goes in v1:
time: 81.9 us; the launch traced here: 81.7 us
  Pallas kernels  79.8 us (97%)
  local copies, waits for them, and re-layouts  1.88 us (2%)
    pallas_call x1, Pallas kernels, fused(): pl.pallas_call(kernel, out_shape=jax.ShapeDtypeStruct((tok_count, width),...  79.8 us
    unnamed x1, local copies, waits for them, and re-layouts  1.88 us

profile of v1, /device:TPU:10, one launch (start us, length us, event | category | flops | bytes accessed | tf_op | source)
XLA Modules:
  0.0 81.7 jit_solution(8636381496323109685)
XLA Ops:
  0.0 79.8 %experts.1 = bf16[128,2048]{1,0:T(8,128)(2,1)} custom-call(s32[2,128]{1,0:T(2,128)} %bitcast.10, f32[2,128]{1,0:T(2,128)} %bitcast.11, f32[1,2048]{1,0:T(1,128)} %bitcast.9, bf16[128,2048]{1,0:T(8,128)(2,1)} %tokens_ref.1, bf16[2048,768]{1,0:T(8,128)(2,1)} %bitcast.6, bf16[2048,768]{1,0:T(8,128)(2,1)} %bitcast.7, bf16[768,2048]{1,0:T(8,128)(2,1)} %bitcast.8), custom_call_target="tpu_custom_call" | custom-call | tf_op jit(solution)/shard_map/experts/pallas_call | solution.py:355
  79.8 1.9 %copy.9 = bf16[128,2048]{1,0:T(8,128)(2,1)} copy(bf16[128,2048]{1,0:T(8,128)(2,1)} %experts.1) | data formatting | bytes 1048576

commit v2 on v1

v2 whole, which is shorter than its diff:
```python
import functools

import jax
import jax.numpy as jnp
from jax import lax
from jax.experimental import pallas as pl
from jax.experimental.pallas import tpu as pltpu
from jax.sharding import PartitionSpec as P

MESH = pl.DeviceIdType.MESH
LINE = 4
PARTS = 4
BANDS = 2

OUTER_TURNS = (0, -1, -3, -2)
INNER_TURNS = (0, 1, -2, -1)
OUTER_PLAN = (
    7000, 7001, 7002, 7003, 7010, 7011, 7012, 7013, 0, 1, 2, 3, 10, 11, 12, 13,
    5000, 5010, 1000, 100, 5100, 1001, 1002, 101, 1003, 1010, 102, 1011, 1012, 103, 1013, 1100,
    300, 5300, 1101, 1102, 301, 1103, 1300, 302, 2100, 303, 1301, 3100, 310, 1302, 5310, 4100,
    4101, 311, 1303, 2300, 312, 313, 6100, 6101, 3300, 200, 6102, 6103, 201, 4300, 4301, 5200,
    1310, 1311, 1312, 1313, 202, 1200, 2310, 203, 6300, 6301, 1201, 3310, 210, 4310, 211, 4311,
    6302, 6303, 1202, 1203, 5210, 212, 2200, 213, 6310, 6311, 110, 1210, 1211, 3200, 111, 4200,
    6312, 4201, 6313, 1212, 5110, 112, 1213, 1110, 113, 2210, 6200, 6201, 3210, 6202, 6203, 4210,
    4211, 1111, 1112, 1113, 2110, 6210, 6211, 3110, 6212, 4110, 6213, 4111, 2000, 6110, 3000, 6111,
    6112, 6113, 4000, 4001, 9000, 9001, 9002, 9003, 4010, 9010, 9011, 4011, 9012, 9013, 6000, 6001,
    6002, 6003, 6010, 6011, 6012, 6013,
)
INNER_PLAN = (
    7000, 8000, 7001, 8001, 7002, 8002, 7003, 0, 5000, 1, 2, 3, 10, 5010, 11, 12,
    13, 8003, 8010, 8011, 8012, 8013, 1000, 300, 5300, 1001, 100, 5100, 1002, 301, 101, 1003,
    1010, 302, 102, 1011, 1012, 303, 103, 1013, 1300, 310, 5310, 1100, 110, 5110, 1301, 311,
    111, 1101, 1302, 312, 112, 1102, 1303, 313, 113, 1103, 2300, 200, 2100, 201, 202, 3100,
    203, 4100, 5200, 4101, 1110, 1111, 1112, 1113, 3300, 2110, 4300, 4301, 210, 5210, 211, 212,
    1200, 1201, 1202, 1203, 1310, 1311, 1312, 1313, 3110, 213, 7010, 7011, 7012, 7013, 4110, 2310,
    4111, 3310, 6300, 4310, 2200, 6301, 4311, 3200, 6302, 4200, 6303, 4201, 1210, 1211, 1212, 1213,
    2000, 6310, 6311, 3000, 6312, 4000, 4001, 2210, 6313, 3210, 6200, 4210, 4010, 4211, 9000, 9001,
    9002, 9003, 6201, 9010, 9011, 4011, 9012, 9013, 6202, 6100, 6203, 6101, 6210, 6000, 6102, 6211,
    6001, 6002, 6103, 6212, 6003, 6110, 6213, 6111, 6010, 6112, 6011, 6113, 6012, 6013,
)


def shards(tokens, norm_gain, expert_ids, route_weights, gate_proj, linear_proj, down_proj):
    tok_count, width = tokens.shape
    picks = expert_ids.shape[1]
    experts = lax.axis_size("ep")
    capacity = 2 * tok_count * picks // experts
    values = tokens.astype(jnp.float32)
    normed = (
        values * lax.rsqrt(jnp.mean(values * values, axis=-1, keepdims=True) + 1e-06) * norm_gain
    ).astype(jnp.bfloat16)
    flat = expert_ids.reshape(-1)
    onehot = (flat[:, None] == jnp.arange(experts, dtype=jnp.int32)[None, :]).astype(jnp.int32)
    slots = jnp.sum((jnp.cumsum(onehot, axis=0) - 1) * onehot, axis=1)
    where = flat * capacity + slots
    buffer = (
        jnp.zeros((experts * capacity, width), jnp.bfloat16)
        .at[where]
        .set(jnp.repeat(normed, picks, axis=0))
    )
    arrived = lax.all_to_all(buffer, "ep", split_axis=0, concat_axis=0, tiled=True)
    rows = lax.all_gather(arrived, "tp", axis=0, tiled=True)
    gate_pre = jnp.dot(rows, gate_proj[0], preferred_element_type=jnp.float32)
    lin_pre = jnp.dot(rows, linear_proj[0], preferred_element_type=jnp.float32)
    glu = jnp.minimum(gate_pre, 7.0)
    lin = jnp.clip(lin_pre, -7.0, 7.0)
    hidden = (glu * jax.nn.sigmoid(1.702 * glu) * (lin + 1.0)).astype(jnp.bfloat16)
    rows = hidden
    summed = lax.psum_scatter(
        jnp.dot(rows, down_proj[0], preferred_element_type=jnp.float32).astype(jnp.bfloat16),
        "tp",
        scatter_dimension=0,
        tiled=True,
    )
    returned = lax.all_to_all(summed, "ep", split_axis=0, concat_axis=0, tiled=True)
    picked = returned[where].reshape(tok_count, picks, width).astype(jnp.float32)
    return jnp.sum(picked * route_weights[:, :, None], axis=1).astype(jnp.bfloat16)


def kernel(
    ids_ref, weights_ref, gain_ref, tokens_hbm, gate_hbm, linear_hbm, down_hbm, out_ref,
    tokens_ref, gate, linear, down, mate, tok, meta, pick, spread, shares, rows, cross, hidden, part, part_in, done,
    back_in, ret_in, ret_out, last, last_in,
    load_sem, mate_send, mate_recv, tok_send, tok_recv, meta_send, meta_recv, cross_send, cross_recv,
    pair_send, pair_recv, part_send, part_recv, back_send, back_recv, ret_send, ret_recv,
    last_send, last_recv,
):
    ep, core = lax.axis_index("ep"), lax.axis_index("tp")
    z, y = ep // 2, ep % 2
    experts = 2 * LINE
    tok_count, width = tokens_hbm.shape
    half = width // 2
    capacity = cross.shape[2]
    ff = gate.shape[1]
    step_cols, step_band, unit = half // PARTS, half // BANDS, 256
    cols = [pl.ds(i * step_cols, step_cols) for i in range(PARTS)]
    here, there = z * 2 + y, z * 2 + 1 - y
    mine = pl.ds(pl.multiple_of(core * half, half), half)
    other = pl.ds(pl.multiple_of((1 - core) * half, half), half)
    at_y = {"ep": there}
    at_core = {"tp": 1 - core}
    outwards = jnp.where(z < LINE // 2, -1, 1)
    outer = (z == 0) | (z == LINE - 1)

    def at_z(other):
        return {"ep": other * 2 + y}

    def remote(source, target, send, recv, device):
        return pltpu.make_async_remote_copy(
            src_ref=source, dst_ref=target, send_sem=send, recv_sem=recv,
            device_id=device, device_id_type=MESH,
        )

    peers = [at_core] + [
        {"ep": lax.rem(z + step, LINE) * 2 + y, "tp": tp} for step in range(1, LINE) for tp in range(2)
    ]
    loads = [
        pltpu.make_async_copy(source, target, load_sem.at[i])
        for i, (source, target) in enumerate(((gate_hbm, gate), (linear_hbm, linear), (down_hbm, down)))
    ]
    fetch = pltpu.make_async_copy(tokens_hbm, tokens_ref, load_sem.at[3])
    fetch.start()
    barrier = pltpu.get_barrier_semaphore()
    for device in peers + [at_y]:
        pl.semaphore_signal(barrier, 1, device_id=device, device_id_type=MESH)

    def normalize(i, _):
        span = pl.ds(pl.multiple_of(i * 32, 32), 32)
        values = tokens_ref[span, :].astype(jnp.float32)
        scale = lax.rsqrt(jnp.mean(values * values, axis=-1, keepdims=True) + 1e-06)
        mate[span, :] = (tokens_ref[span, other].astype(jnp.float32) * scale * gain_ref[:, other]).astype(
            jnp.bfloat16
        )
        tok[z, core, span, :] = (tokens_ref[span, mine].astype(jnp.float32) * scale * gain_ref[:, mine]).astype(
            jnp.bfloat16
        )
        return 0

    fetch.wait()
    for load in loads:
        load.start()
    lax.fori_loop(0, tok_count // 32, normalize, 0)
    pl.semaphore_wait(barrier, len(peers) + 1)
    mate_copy = remote(mate, tok.at[z, core], mate_send.at[0], mate_recv.at[0], at_core)
    mate_copy.start()
    names = lax.broadcasted_iota(jnp.int32, (experts, tok_count), 0)
    share = jnp.zeros((experts, tok_count), jnp.float32)
    chosen = jnp.zeros((experts, tok_count), jnp.float32)
    for choice in range(ids_ref.shape[0]):
        same = ids_ref[choice : choice + 1, :] == names
        share = share + jnp.where(same, weights_ref[choice : choice + 1, :], 0.0)
        chosen = chosen + jnp.where(same, 1.0, 0.0)
    first = lax.broadcasted_iota(jnp.int32, (tok_count, tok_count), 0)
    second = lax.broadcasted_iota(jnp.int32, (tok_count, tok_count), 1)
    before = jnp.where(first < second, 1.0, 0.0).astype(jnp.bfloat16)
    slots = jnp.dot(chosen.astype(jnp.bfloat16), before, preferred_element_type=jnp.float32)
    meta[z, core, 0:experts, :] = jnp.where(chosen > 0.5, slots, -1.0)
    meta[z, core, experts : 2 * experts, :] = share

    def meta_copy(k):
        block = meta.at[z, core]
        return remote(block, block, meta_send.at[k], meta_recv.at[z, core], peers[k])

    def meta_arrival(source, h):
        block = meta.at[source, h]
        return remote(block, block, meta_send.at[0], meta_recv.at[source, h], at_core)

    def hop(source, h, i, way):
        block = tok.at[source, h, :, cols[i]]
        target = z + outwards if way else z - outwards
        return remote(
            block, block, tok_send.at[source, h, i, way], tok_recv.at[source, h, i], at_z(target)
        )

    def cross_copy(source, h, i):
        return remote(
            cross.at[source, h, :, cols[i]], rows.at[source, h, core, y, :, cols[i]],
            cross_send.at[source, h, i], cross_recv.at[source, h, i], at_y,
        )

    def cross_arrival(source, h, i):
        return remote(
            cross.at[source, h, :, cols[i]], rows.at[source, h, core, 1 - y, :, cols[i]],
            cross_send.at[source, h, i], cross_recv.at[source, h, i], at_y,
        )

    def pair_move(source, h, owner, column, i):
        block = rows.at[source, h, owner, column, :, cols[i]]
        return remote(
            block, block, pair_send.at[source, h, column, i], pair_recv.at[source, h, column, i], at_core
        )

    def part_copy(source, h, i):
        band = pl.ds(i * step_band, step_band) if isinstance(i, int) else pl.ds(
            pl.multiple_of(i * step_band, step_band), step_band
        )
        return remote(
            part.at[source, h, 1 - core, :, :, band], part_in.at[source, h, :, :, band],
            part_send.at[source, h, i], part_recv.at[source, h, i], at_core,
        )

    def back_copy(source, h, i):
        return remote(
            done.at[source, h, 1 - y, :, cols[i]], back_in.at[source, h, :, cols[i]],
            back_send.at[source, h, i], back_recv.at[source, h, i], at_y,
        )

    def ret_copy(source, h, i, way):
        step = outwards if way else -outwards
        side = jnp.where(step > 0, 0, 1)
        return remote(
            ret_out.at[source, h, :, cols[i]], ret_in.at[side, source, h, :, cols[i]],
            ret_send.at[source, h, i], ret_recv.at[side, source, h, i], at_z(z + step),
        )

    def ret_arrival(source, h, i, way):
        step = -outwards if way else outwards
        side = jnp.where(step > 0, 0, 1)
        return side, remote(
            ret_out.at[source, h, :, cols[i]], ret_in.at[side, source, h, :, cols[i]],
            ret_send.at[source, h, i], ret_recv.at[side, source, h, i], at_z(z - step),
        )

    def last_copy(h, i):
        return remote(
            last.at[h, :, cols[i]], last_in.at[:, cols[i]], last_send.at[i], last_recv.at[i], at_core
        )

    def run(plan, turns, at_end):
        order = [z + outwards * turn for turn in turns]
        if at_end:
            passes = [(0,), (), (), ()]
            comes = [(0,), (), (), ()]
        else:
            passes = [(1, 0)] + [(0,) if turn > 0 else (1,) for turn in turns[1:]]
            comes = [(0, 1)] + [(0,) if turn > 0 else (1,) for turn in turns[1:]]
        leaves = [None] + [1 if turn > 0 else 0 for turn in turns[1:]]
        waited = [False, False]

        def send_rows(t, h, i):
            source = order[t]
            if t:
                hop(source, h, i, 0).wait_recv()
                for way in passes[t]:
                    hop(source, h, i, way).start()
            if i == 0:
                if t:
                    meta_arrival(source, h).wait_recv()
                place = lax.broadcasted_iota(jnp.int32, (capacity, tok_count), 0).astype(jnp.float32)
                for k, expert in enumerate((there, here)):
                    pick[t, h, k * capacity : (k + 1) * capacity, :] = (
                        meta[source, h, pl.ds(expert, 1), :] == place
                    ).astype(jnp.bfloat16)
            both = jnp.dot(
                pick[t, h], tok[source, h, :, cols[i]], preferred_element_type=jnp.float32
            ).astype(jnp.bfloat16)
            cross[source, h, :, cols[i]] = both[:capacity]
            cross_copy(source, h, i).start()
            rows[source, h, core, y, :, cols[i]] = both[capacity:]
            pair_move(source, h, core, y, i).start()

        def share_rows(t, h, i):
            source = order[t]
            cross_arrival(source, h, i).wait_recv()
            pair_move(source, h, core, 1 - y, i).start()

        def up(t, h, i):
            source = order[t]
            blocks = range(h, h + 1) if t else range(2)
            for block in blocks:
                for column in range(2):
                    for j in range(PARTS):
                        pair_move(source, block, 1 - core, column, j).wait_recv()
            if not waited[0]:
                waited[0] = True
                loads[0].wait()
                loads[1].wait()
            span_h = slice(blocks[0], blocks[-1] + 1)

            def units(j, _):
                span = pl.ds(pl.multiple_of(j * unit, unit), unit)
                low = rows[source, span_h, 0].reshape(len(blocks) * 2 * capacity, half)
                high = rows[source, span_h, 1].reshape(len(blocks) * 2 * capacity, half)

                def through(matrix):
                    return jnp.dot(low, matrix[:half, span], preferred_element_type=jnp.float32) + jnp.dot(
                        high, matrix[half:, span], preferred_element_type=jnp.float32
                    )

                glu = jnp.minimum(through(gate), 7.0)
                lin = jnp.clip(through(linear), -7.0, 7.0)
                hidden[t, span_h, :, span] = (
                    (glu * jax.nn.sigmoid(1.702 * glu) * (lin + 1.0))
                    .astype(jnp.bfloat16)
                    .reshape(len(blocks), 2 * capacity, unit)
                )
                return 0

            lax.fori_loop(0, ff // unit, units, 0)

        def out(t, h, i):
            source = order[t]
            blocks = range(h, h + 1) if t else range(2)
            span_h = slice(blocks[0], blocks[-1] + 1)
            if not waited[1]:
                waited[1] = True
                loads[2].wait()

            def bands(side, send):
                def go(j, _):
                    start = side * half + j * step_band
                    span = pl.ds(pl.multiple_of(start, step_band), step_band)
                    inputs = hidden[t, span_h].reshape(len(blocks) * 2 * capacity, ff)
                    part[source, span_h, side, :, :, pl.ds(pl.multiple_of(j * step_band, step_band), step_band)] = (
                        jnp.dot(inputs, down[:, span], preferred_element_type=jnp.float32)
                        .astype(jnp.bfloat16)
                        .reshape(len(blocks), 2, capacity, step_band)
                    )
                    if send:
                        for block in blocks:
                            part_copy(source, block, j).start()
                    return 0

                lax.fori_loop(0, BANDS, go, 0)

            bands(1 - core, True)
            bands(core, False)

        def add(t, h, i):
            source = order[t]
            part_copy(source, h, i).wait_recv()
            band = pl.ds(i * step_band, step_band)
            done[source, h, :, :, band] = (
                part[source, h, core, :, :, band].astype(jnp.float32)
                + part_in[source, h, :, :, band].astype(jnp.float32)
            ).astype(jnp.bfloat16)
            if t:
                for j in range(i * PARTS // BANDS, (i + 1) * PARTS // BANDS):
                    back_copy(source, h, j).start()

        def turn_over(t, h, i):
            source = order[t]
            eye = lax.broadcasted_iota(jnp.int32, (tok_count, tok_count), 0) == lax.broadcasted_iota(
                jnp.int32, (tok_count, tok_count), 1
            )
            lane = lax.broadcasted_iota(jnp.int32, (tok_count, capacity), 1).astype(jnp.float32)

            def upright(row):
                return jnp.sum(jnp.where(eye, meta[source, h, pl.ds(row, 1), :], 0.0), axis=1, keepdims=True)

            for k, expert in enumerate((here, there)):
                spread[t, h, k] = (upright(expert) == lane).astype(jnp.bfloat16)
                shares[t, h, k] = jnp.broadcast_to(upright(experts + expert), (tok_count, 128))

        def merge(t, h, i):
            source = order[t]
            back_copy(source, h, i).wait_recv()
            total = None
            for k, block in enumerate((done[source, h, y, :, cols[i]], back_in[source, h, :, cols[i]])):
                scale = jnp.concatenate([shares[t, h, k]] * (step_cols // 128), axis=1)
                term = scale * jnp.dot(spread[t, h, k], block, preferred_element_type=jnp.float32)
                total = term if total is None else total + term
            for way in comes[t]:
                side, arrival = ret_arrival(source, h, i, way)
                arrival.wait_recv()
                total = total + ret_in[side, source, h, :, cols[i]].astype(jnp.float32)
            if t:
                ret_out[source, h, :, cols[i]] = total.astype(jnp.bfloat16)
                ret_copy(source, h, i, leaves[t]).start()
            else:
                last[h, :, cols[i]] = total.astype(jnp.bfloat16)
                pl.when(core != h)(lambda: last_copy(h, i).start())

        def near(t, h, i):
            hop(z, h, i, 0 if at_end else 1).start()

        def far(t, h, i):
            hop(z, h, i, 0).start()

        def own_back(t, h, i):
            back_copy(z, h, i).start()

        stages = (send_rows, share_rows, up, out, add, turn_over, merge, near, far, own_back)
        for number in plan:
            stages[number // 1000](number // 100 % 10, number // 10 % 10, number % 10)
        for t in range(LINE):
            source = order[t]
            for h in range(2):
                for i in range(PARTS):
                    for way in passes[t]:
                        hop(source, h, i, way).wait_send()
                    cross_copy(source, h, i).wait_send()
                    for column in range(2):
                        pair_move(source, h, core, column, i).wait_send()
                    back_copy(source, h, i).wait_send()
                    if t:
                        ret_copy(source, h, i, leaves[t]).wait_send()
                for i in range(BANDS):
                    part_copy(source, h, i).wait_send()

    for k in range(len(peers)):
        meta_copy(k).start()
    mate_copy.wait_recv()
    meta_arrival(z, 1 - core).wait_recv()
    pl.when(outer)(lambda: run(OUTER_PLAN, OUTER_TURNS, True))
    pl.when(jnp.logical_not(outer))(lambda: run(INNER_PLAN, INNER_TURNS, False))
    out_ref[:, mine] = last[core]
    for i in range(PARTS):
        last_copy(1 - core, i).wait_recv()
    out_ref[:, other] = last_in[...]
    mate_copy.wait_send()
    for k in range(len(peers)):
        meta_copy(k).wait_send()
    for i in range(PARTS):
        last_copy(1 - core, i).wait_send()


def fused(tokens, norm_gain, expert_ids, route_weights, gate_proj, linear_proj, down_proj):
    tok_count, width = tokens.shape
    picks = expert_ids.shape[1]
    experts = 2 * LINE
    capacity = 2 * tok_count * picks // experts
    ff = gate_proj.shape[2]
    wide, dma = jnp.bfloat16, pltpu.SemaphoreType.DMA
    inside, outside = pl.BlockSpec(memory_space=pltpu.VMEM), pl.BlockSpec(memory_space=pl.ANY)
    return pl.pallas_call(
        kernel,
        out_shape=jax.ShapeDtypeStruct((tok_count, width), wide),
        in_specs=[inside] * 3 + [outside] * 4,
        out_specs=inside,
        scratch_shapes=[
            pltpu.VMEM((tok_count, width), wide),
            pltpu.VMEM((width, ff), wide),
            pltpu.VMEM((width, ff), wide),
            pltpu.VMEM((ff, width), wide),
            pltpu.VMEM((tok_count, width // 2), wide),
            pltpu.VMEM((LINE, 2, tok_count, width // 2), wide),
            pltpu.VMEM((LINE, 2, 2 * experts, tok_count), jnp.float32),
            pltpu.VMEM((LINE, 2, 2 * capacity, tok_count), wide),
            pltpu.VMEM((LINE, 2, 2, tok_count, capacity), wide),
            pltpu.VMEM((LINE, 2, 2, tok_count, 128), jnp.float32),
            pltpu.VMEM((LINE, 2, 2, 2, capacity, width // 2), wide),
            pltpu.VMEM((LINE, 2, capacity, width // 2), wide),
            pltpu.VMEM((LINE, 2, 2 * capacity, ff), wide),
            pltpu.VMEM((LINE, 2, 2, 2, capacity, width // 2), wide),
            pltpu.VMEM((LINE, 2, 2, capacity, width // 2), wide),
            pltpu.VMEM((LINE, 2, 2, capacity, width // 2), wide),
            pltpu.VMEM((LINE, 2, capacity, width // 2), wide),
            pltpu.VMEM((2, LINE, 2, tok_count, width // 2), wide),
            pltpu.VMEM((LINE, 2, tok_count, width // 2), wide),
            pltpu.VMEM((2, tok_count, width // 2), wide),
            pltpu.VMEM((tok_count, width // 2), wide),
            dma((4,)),
            dma((1,)), dma((1,)),
            dma((LINE, 2, PARTS, 2)), dma((LINE, 2, PARTS)),
            dma((2 * LINE - 1,)), dma((LINE, 2)),
            dma((LINE, 2, PARTS)), dma((LINE, 2, PARTS)),
            dma((LINE, 2, 2, PARTS)), dma((LINE, 2, 2, PARTS)),
            dma((LINE, 2, BANDS)), dma((LINE, 2, BANDS)),
            dma((LINE, 2, PARTS)), dma((LINE, 2, PARTS)),
            dma((LINE, 2, PARTS)), dma((2, LINE, 2, PARTS)),
            dma((PARTS,)), dma((PARTS,)),
        ],
        compiler_params=pltpu.CompilerParams(
            collective_id=0, has_side_effects=True, vmem_limit_bytes=60 * 1024 * 1024
        ),
        name="experts",
    )(
        expert_ids.T, route_weights.T, norm_gain.reshape(1, width), tokens,
        gate_proj[0], linear_proj[0], down_proj[0],
    )


def solution(mesh):
    placed = (
        P(("grp", "ep", "tp"), None),
        P(),
        P(("grp", "ep", "tp"), None),
        P(("grp", "ep", "tp"), None),
        P("ep", None, "tp"),
        P("ep", None, "tp"),
        P("ep", "tp", None),
    )
    along = [device.coords[2] for device in mesh.devices[0, :, 0]]
    planned = along == [index // 2 for index in range(2 * LINE)] and mesh.shape["tp"] == 2
    return jax.shard_map(
        fused if planned else shards,
        mesh=mesh,
        in_specs=placed,
        out_specs=P(("grp", "ep", "tp"), None),
        check_vma=False,
    )
```

time: 81.9 us -> 75.7 us (0.924)
  the two profiles are of different devices: /device:TPU:10 before, /device:TPU:0 now
where the time goes in v2:
time: 75.7 us; the launch traced here: 75.4 us
  Pallas kernels  73.5 us (97%)
  local copies, waits for them, and re-layouts  1.88 us (2%)
    pallas_call x1, Pallas kernels, fused(): pl.pallas_call(kernel, out_shape=jax.ShapeDtypeStruct((tok_count, width),...  73.5 us
    unnamed x1, local copies, waits for them, and re-layouts  1.88 us

profile of v2, /device:TPU:0, one launch (start us, length us, event | category | flops | bytes accessed | tf_op | source)
XLA Modules:
  0.0 75.4 jit_solution(15272145390678547487)
XLA Ops:
  0.0 73.5 %experts.1 = bf16[128,2048]{1,0:T(8,128)(2,1)} custom-call(s32[2,128]{1,0:T(2,128)} %bitcast.10, f32[2,128]{1,0:T(2,128)} %bitcast.11, f32[1,2048]{1,0:T(1,128)} %bitcast.9, bf16[128,2048]{1,0:T(8,128)(2,1)} %tokens_hbm.1, bf16[2048,768]{1,0:T(8,128)(2,1)} %bitcast.6, bf16[2048,768]{1,0:T(8,128)(2,1)} %bitcast.7, bf16[768,2048]{1,0:T(8,128)(2,1)} %bitcast.8), custom_call_target="tpu_custom_call" | custom-call | tf_op jit(solution)/shard_map/experts/pallas_call | solution.py:426
  73.5 1.9 %copy.9 = bf16[128,2048]{1,0:T(8,128)(2,1)} copy(bf16[128,2048]{1,0:T(8,128)(2,1)} %experts.1) | data formatting | bytes 1048576

commit v3 on v2

--- a/solution.py
+++ b/solution.py
@@ -10,33 +10,36 @@
 MESH = pl.DeviceIdType.MESH
 LINE = 4
 PARTS = 4
+SETTLE = 2
 BANDS = 2
 
 OUTER_TURNS = (0, -1, -3, -2)
 INNER_TURNS = (0, 1, -2, -1)
 OUTER_PLAN = (
-    7000, 7001, 7002, 7003, 7010, 7011, 7012, 7013, 0, 1, 2, 3, 10, 11, 12, 13,
-    5000, 5010, 1000, 100, 5100, 1001, 1002, 101, 1003, 1010, 102, 1011, 1012, 103, 1013, 1100,
-    300, 5300, 1101, 1102, 301, 1103, 1300, 302, 2100, 303, 1301, 3100, 310, 1302, 5310, 4100,
-    4101, 311, 1303, 2300, 312, 313, 6100, 6101, 3300, 200, 6102, 6103, 201, 4300, 4301, 5200,
-    1310, 1311, 1312, 1313, 202, 1200, 2310, 203, 6300, 6301, 1201, 3310, 210, 4310, 211, 4311,
-    6302, 6303, 1202, 1203, 5210, 212, 2200, 213, 6310, 6311, 110, 1210, 1211, 3200, 111, 4200,
-    6312, 4201, 6313, 1212, 5110, 112, 1213, 1110, 113, 2210, 6200, 6201, 3210, 6202, 6203, 4210,
-    4211, 1111, 1112, 1113, 2110, 6210, 6211, 3110, 6212, 4110, 6213, 4111, 2000, 6110, 3000, 6111,
-    6112, 6113, 4000, 4001, 9000, 9001, 9002, 9003, 4010, 9010, 9011, 4011, 9012, 9013, 6000, 6001,
-    6002, 6003, 6010, 6011, 6012, 6013,
+    7000, 7001, 7002, 7003, 7010, 7011, 7012, 7013, 10, 11, 12, 13, 5010, 0, 5000, 1,
+    2, 3, 1010, 100, 5100, 1011, 1012, 101, 1013, 1000, 102, 1001, 1002, 103, 1003, 1100,
+    300, 5300, 1101, 2000, 301, 1102, 1103, 2001, 3000, 302, 1300, 2100, 303, 2101, 1301, 3100,
+    310, 3101, 1302, 4100, 5310, 4101, 311, 3001, 4010, 4011, 1303, 4000, 4001, 312, 1310, 2300,
+    313, 6100, 6101, 2301, 3300, 200, 3301, 6102, 6103, 1311, 4300, 201, 5200, 4301, 1312, 1313,
+    202, 1200, 2310, 203, 6300, 2311, 6301, 3310, 1201, 210, 3311, 6302, 211, 5210, 4310, 6303,
+    4311, 1202, 212, 1203, 1210, 213, 2200, 1211, 6310, 2201, 110, 6311, 3200, 6312, 111, 3201,
+    6313, 4200, 1212, 4201, 5110, 112, 1213, 1110, 113, 2210, 1111, 6200, 2211, 3210, 6201, 6202,
+    3211, 6203, 4210, 4211, 1112, 1113, 2110, 6210, 2111, 6211, 3110, 6212, 3111, 6213, 4110, 4111,
+    9000, 9001, 9002, 9003, 9010, 9011, 9012, 9013, 6110, 6111, 6112, 6113, 6000, 6001, 6002, 6003,
+    6010, 6011, 6012, 6013,
 )
 INNER_PLAN = (
-    7000, 8000, 7001, 8001, 7002, 8002, 7003, 0, 5000, 1, 2, 3, 10, 5010, 11, 12,
-    13, 8003, 8010, 8011, 8012, 8013, 1000, 300, 5300, 1001, 100, 5100, 1002, 301, 101, 1003,
-    1010, 302, 102, 1011, 1012, 303, 103, 1013, 1300, 310, 5310, 1100, 110, 5110, 1301, 311,
-    111, 1101, 1302, 312, 112, 1102, 1303, 313, 113, 1103, 2300, 200, 2100, 201, 202, 3100,
-    203, 4100, 5200, 4101, 1110, 1111, 1112, 1113, 3300, 2110, 4300, 4301, 210, 5210, 211, 212,
-    1200, 1201, 1202, 1203, 1310, 1311, 1312, 1313, 3110, 213, 7010, 7011, 7012, 7013, 4110, 2310,
-    4111, 3310, 6300, 4310, 2200, 6301, 4311, 3200, 6302, 4200, 6303, 4201, 1210, 1211, 1212, 1213,
-    2000, 6310, 6311, 3000, 6312, 4000, 4001, 2210, 6313, 3210, 6200, 4210, 4010, 4211, 9000, 9001,
-    9002, 9003, 6201, 9010, 9011, 4011, 9012, 9013, 6202, 6100, 6203, 6101, 6210, 6000, 6102, 6211,
-    6001, 6002, 6103, 6212, 6003, 6110, 6213, 6111, 6010, 6112, 6011, 6113, 6012, 6013,
+    7000, 8000, 7001, 8001, 7002, 8002, 7003, 0, 1, 2, 3, 8003, 8010, 8011, 8012, 8013,
+    10, 11, 12, 13, 5000, 5010, 1000, 100, 300, 5300, 5100, 1001, 1002, 101, 301, 1003,
+    1010, 102, 302, 1011, 1012, 103, 303, 1013, 1100, 310, 110, 5310, 1300, 5110, 2000, 311,
+    111, 1301, 1101, 2001, 1102, 112, 312, 3000, 1302, 1103, 3001, 313, 113, 1303, 4010, 4000,
+    4001, 1310, 4011, 2100, 200, 2101, 1311, 2300, 201, 2301, 3300, 1312, 202, 3301, 1313, 1110,
+    1111, 1112, 203, 4300, 5200, 4301, 1113, 3100, 2310, 210, 2311, 1200, 1201, 1202, 3310, 211,
+    1203, 3311, 212, 4310, 5210, 4311, 2110, 2200, 2201, 213, 7010, 7011, 7012, 7013, 1210, 3200,
+    1211, 3201, 1212, 2111, 4200, 4201, 3110, 3111, 6300, 3101, 4100, 4101, 4110, 4111, 9000, 9001,
+    9002, 9003, 9010, 9011, 9012, 9013, 6301, 1213, 6302, 2210, 2211, 6303, 3210, 3211, 4210, 6310,
+    4211, 6311, 6312, 6313, 6000, 6001, 6200, 6002, 6003, 6201, 6202, 6100, 6203, 6101, 6210, 6102,
+    6211, 6103, 6212, 6110, 6213, 6111, 6010, 6112, 6011, 6113, 6012, 6013,
 )
 
 
@@ -78,8 +81,8 @@
 
 
 def kernel(
-    ids_ref, weights_ref, gain_ref, tokens_hbm, gate_hbm, linear_hbm, down_hbm, out_ref,
-    tokens_ref, gate, linear, down, mate, tok, meta, pick, spread, shares, rows, cross, hidden, part, part_in, done,
+    ids_hbm, weights_hbm, gain_hbm, tokens_hbm, gate_hbm, linear_hbm, down_hbm, out_ref,
+    ids_ref, weights_ref, gain_ref, tokens_ref, gate, linear, down, mate, tok, meta, pick, spread, shares, rows, cross, hidden, part, part_in, done,
     back_in, ret_in, ret_out, last, last_in,
     load_sem, mate_send, mate_recv, tok_send, tok_recv, meta_send, meta_recv, cross_send, cross_recv,
     pair_send, pair_recv, part_send, part_recv, back_send, back_recv, ret_send, ret_recv,
@@ -94,6 +97,7 @@
     ff = gate.shape[1]
     step_cols, step_band, unit = half // PARTS, half // BANDS, 256
     cols = [pl.ds(i * step_cols, step_cols) for i in range(PARTS)]
+    whole = pl.ds(0, half)
     here, there = z * 2 + y, z * 2 + 1 - y
     mine = pl.ds(pl.multiple_of(core * half, half), half)
     other = pl.ds(pl.multiple_of((1 - core) * half, half), half)
@@ -118,8 +122,14 @@
         pltpu.make_async_copy(source, target, load_sem.at[i])
         for i, (source, target) in enumerate(((gate_hbm, gate), (linear_hbm, linear), (down_hbm, down)))
     ]
-    fetch = pltpu.make_async_copy(tokens_hbm, tokens_ref, load_sem.at[3])
-    fetch.start()
+    fetches = [
+        pltpu.make_async_copy(source, target, load_sem.at[3 + i])
+        for i, (source, target) in enumerate(
+            ((tokens_hbm, tokens_ref), (gain_hbm, gain_ref), (ids_hbm, ids_ref), (weights_hbm, weights_ref))
+        )
+    ]
+    for fetch in fetches:
+        fetch.start()
     barrier = pltpu.get_barrier_semaphore()
     for device in peers + [at_y]:
         pl.semaphore_signal(barrier, 1, device_id=device, device_id_type=MESH)
@@ -136,7 +146,8 @@
         )
         return 0
 
-    fetch.wait()
+    for fetch in fetches:
+        fetch.wait()
     for load in loads:
         load.start()
     lax.fori_loop(0, tok_count // 32, normalize, 0)
@@ -165,52 +176,59 @@
         block = meta.at[source, h]
         return remote(block, block, meta_send.at[0], meta_recv.at[source, h], at_core)
 
+    def piece(i):
+        return whole if i is None else cols[i]
+
+    def first(i):
+        return 0 if i is None else i
+
     def hop(source, h, i, way):
-        block = tok.at[source, h, :, cols[i]]
+        block = tok.at[source, h, :, piece(i)]
         target = z + outwards if way else z - outwards
         return remote(
-            block, block, tok_send.at[source, h, i, way], tok_recv.at[source, h, i], at_z(target)
+            block, block, tok_send.at[source, h, way], tok_recv.at[source, h, first(i)], at_z(target)
         )
 
     def cross_copy(source, h, i):
         return remote(
-            cross.at[source, h, :, cols[i]], rows.at[source, h, core, y, :, cols[i]],
-            cross_send.at[source, h, i], cross_recv.at[source, h, i], at_y,
+            cross.at[source, h, :, piece(i)], rows.at[source, h, core, y, :, piece(i)],
+            cross_send.at[source, h], cross_recv.at[source, h, first(i)], at_y,
         )
 
     def cross_arrival(source, h, i):
         return remote(
             cross.at[source, h, :, cols[i]], rows.at[source, h, core, 1 - y, :, cols[i]],
-            cross_send.at[source, h, i], cross_recv.at[source, h, i], at_y,
-        )
-
-    def pair_move(source, h, owner, column, i):
-        block = rows.at[source, h, owner, column, :, cols[i]]
-        return remote(
-            block, block, pair_send.at[source, h, column, i], pair_recv.at[source, h, column, i], at_core
-        )
+            cross_send.at[source, h], cross_recv.at[source, h, i], at_y,
+        )
+
+    def pair_move(source, h, owner, span):
+        block = rows.at[source, h, owner, :, :, span]
+        return remote(block, block, pair_send.at[source, h], pair_recv.at[source, h], at_core)
 
     def part_copy(source, h, i):
-        band = pl.ds(i * step_band, step_band) if isinstance(i, int) else pl.ds(
-            pl.multiple_of(i * step_band, step_band), step_band
-        )
+        if i is None:
+            band = whole
+        elif isinstance(i, int):
+            band = pl.ds(i * step_band, step_band)
+        else:
+            band = pl.ds(pl.multiple_of(i * step_band, step_band), step_band)
         return remote(
             part.at[source, h, 1 - core, :, :, band], part_in.at[source, h, :, :, band],
-            part_send.at[source, h, i], part_recv.at[source, h, i], at_core,
+            part_send.at[source, h], part_recv.at[source, h, first(i)], at_core,
         )
 
     def back_copy(source, h, i):
         return remote(
-            done.at[source, h, 1 - y, :, cols[i]], back_in.at[source, h, :, cols[i]],
-            back_send.at[source, h, i], back_recv.at[source, h, i], at_y,
+            done.at[source, h, 1 - y, :, piece(i)], back_in.at[source, h, :, piece(i)],
+            back_send.at[source, h], back_recv.at[source, h, first(i)], at_y,
         )
 
     def ret_copy(source, h, i, way):
         step = outwards if way else -outwards
         side = jnp.where(step > 0, 0, 1)
         return remote(
-            ret_out.at[source, h, :, cols[i]], ret_in.at[side, source, h, :, cols[i]],
-            ret_send.at[source, h, i], ret_recv.at[side, source, h, i], at_z(z + step),
+            ret_out.at[source, h, :, piece(i)], ret_in.at[side, source, h, :, piece(i)],
+            ret_send.at[source, h], ret_recv.at[side, source, h, first(i)], at_z(z + step),
         )
 
     def ret_arrival(source, h, i, way):
@@ -218,7 +236,7 @@
         side = jnp.where(step > 0, 0, 1)
         return side, remote(
             ret_out.at[source, h, :, cols[i]], ret_in.at[side, source, h, :, cols[i]],
-            ret_send.at[source, h, i], ret_recv.at[side, source, h, i], at_z(z - step),
+            ret_send.at[source, h], ret_recv.at[side, source, h, i], at_z(z - step),
         )
 
     def last_copy(h, i):
@@ -257,20 +275,17 @@
             cross[source, h, :, cols[i]] = both[:capacity]
             cross_copy(source, h, i).start()
             rows[source, h, core, y, :, cols[i]] = both[capacity:]
-            pair_move(source, h, core, y, i).start()
 
         def share_rows(t, h, i):
             source = order[t]
             cross_arrival(source, h, i).wait_recv()
-            pair_move(source, h, core, 1 - y, i).start()
+            pair_move(source, h, core, cols[i]).start()
 
         def up(t, h, i):
             source = order[t]
             blocks = range(h, h + 1) if t else range(2)
-            for block in blocks:
-                for column in range(2):
-                    for j in range(PARTS):
-                        pair_move(source, block, 1 - core, column, j).wait_recv()
+            for block in blocks if i == 0 else ():
+                pair_move(source, block, 1 - core, whole).wait_recv()
             if not waited[0]:
                 waited[0] = True
                 loads[0].wait()
@@ -278,7 +293,7 @@
             span_h = slice(blocks[0], blocks[-1] + 1)
 
             def units(j, _):
-                span = pl.ds(pl.multiple_of(j * unit, unit), unit)
+                span = pl.ds(j * unit if isinstance(j, int) else pl.multiple_of(j * unit, unit), unit)
                 low = rows[source, span_h, 0].reshape(len(blocks) * 2 * capacity, half)
                 high = rows[source, span_h, 1].reshape(len(blocks) * 2 * capacity, half)
 
@@ -296,7 +311,10 @@
                 )
                 return 0
 
-            lax.fori_loop(0, ff // unit, units, 0)
+            if i == 0:
+                lax.fori_loop(0, ff // unit - 1, units, 0)
+            else:
+                units(ff // unit - 1, 0)
 
         def out(t, h, i):
             source = order[t]
@@ -323,8 +341,7 @@
 
                 lax.fori_loop(0, BANDS, go, 0)
 
-            bands(1 - core, True)
-            bands(core, False)
+            bands(core if i else 1 - core, i == 0)
 
         def add(t, h, i):
             source = order[t]
@@ -380,23 +397,25 @@
         def own_back(t, h, i):
             back_copy(z, h, i).start()
 
+        def settle():
+            for t in range(LINE):
+                source = order[t]
+                for h in range(2):
+                    for way in passes[t]:
+                        hop(source, h, None, way).wait_send()
+                    cross_copy(source, h, None).wait_send()
+                    pair_move(source, h, core, whole).wait_send()
+                    part_copy(source, h, None).wait_send()
+                    back_copy(source, h, None).wait_send()
+
         stages = (send_rows, share_rows, up, out, add, turn_over, merge, near, far, own_back)
-        for number in plan:
+        for place, number in enumerate(plan):
+            if place == len(plan) - SETTLE:
+                settle()
             stages[number // 1000](number // 100 % 10, number // 10 % 10, number % 10)
-        for t in range(LINE):
-            source = order[t]
+        for t in range(1, LINE):
             for h in range(2):
-                for i in range(PARTS):
-                    for way in passes[t]:
-                        hop(source, h, i, way).wait_send()
-                    cross_copy(source, h, i).wait_send()
-                    for column in range(2):
-                        pair_move(source, h, core, column, i).wait_send()
-                    back_copy(source, h, i).wait_send()
-                    if t:
-                        ret_copy(source, h, i, leaves[t]).wait_send()
-                for i in range(BANDS):
-                    part_copy(source, h, i).wait_send()
+                ret_copy(order[t], h, None, leaves[t]).wait_send()
 
     for k in range(len(peers)):
         meta_copy(k).start()
@@ -426,9 +445,12 @@
     return pl.pallas_call(
         kernel,
         out_shape=jax.ShapeDtypeStruct((tok_count, width), wide),
-        in_specs=[inside] * 3 + [outside] * 4,
+        in_specs=[outside] * 7,
         out_specs=inside,
         scratch_shapes=[
+            pltpu.VMEM((picks, tok_count), jnp.int32),
+            pltpu.VMEM((picks, tok_count), jnp.float32),
+            pltpu.VMEM((1, width), jnp.float32),
             pltpu.VMEM((tok_count, width), wide),
             pltpu.VMEM((width, ff), wide),
             pltpu.VMEM((width, ff), wide),
@@ -450,15 +472,15 @@
             pltpu.VMEM((LINE, 2, tok_count, width // 2), wide),
             pltpu.VMEM((2, tok_count, width // 2), wide),
             pltpu.VMEM((tok_count, width // 2), wide),
-            dma((4,)),
+            dma((7,)),
             dma((1,)), dma((1,)),
-            dma((LINE, 2, PARTS, 2)), dma((LINE, 2, PARTS)),
+            dma((LINE, 2, 2)), dma((LINE, 2, PARTS)),
             dma((2 * LINE - 1,)), dma((LINE, 2)),
-            dma((LINE, 2, PARTS)), dma((LINE, 2, PARTS)),
-            dma((LINE, 2, 2, PARTS)), dma((LINE, 2, 2, PARTS)),
-            dma((LINE, 2, BANDS)), dma((LINE, 2, BANDS)),
-            dma((LINE, 2, PARTS)), dma((LINE, 2, PARTS)),
-            dma((LINE, 2, PARTS)), dma((2, LINE, 2, PARTS)),
+            dma((LINE, 2)), dma((LINE, 2, PARTS)),
+            dma((LINE, 2)), dma((LINE, 2)),
+            dma((LINE, 2)), dma((LINE, 2, BANDS)),
+            dma((LINE, 2)), dma((LINE, 2, PARTS)),
+            dma((LINE, 2)), dma((2, LINE, 2, PARTS)),
             dma((PARTS,)), dma((PARTS,)),
         ],
         compiler_params=pltpu.CompilerParams(

time: 75.7 us -> 71.3 us (0.942)
  Pallas kernels: 73.5 us -> 69.3 us
    pallas_call x1, Pallas kernels: 73.5 us -> 69.3 us  [fused(): pl.pallas_call(kernel, out_shape=jax.ShapeDtypeStruct((tok_count, width),...]
where the time goes in v3:
time: 71.3 us; the launch traced here: 71.2 us
  Pallas kernels  69.3 us (97%)
  local copies, waits for them, and re-layouts  1.88 us (3%)
    pallas_call x1, Pallas kernels, fused(): pl.pallas_call(kernel, out_shape=jax.ShapeDtypeStruct((tok_count, width),...  69.3 us
    unnamed x1, local copies, waits for them, and re-layouts  1.88 us

profile of v3, /device:TPU:0, one launch (start us, length us, event | category | flops | bytes accessed | tf_op | source)
XLA Modules:
  0.0 71.2 jit_solution(5511894328617098430)
XLA Ops:
  0.0 69.3 %experts.1 = bf16[128,2048]{1,0:T(8,128)(2,1)} custom-call(s32[2,128]{1,0:T(2,128)} %bitcast.10, f32[2,128]{1,0:T(2,128)} %bitcast.11, f32[1,2048]{1,0:T(1,128)} %bitcast.9, bf16[128,2048]{1,0:T(8,128)(2,1)} %tokens_hbm.1, bf16[2048,768]{1,0:T(8,128)(2,1)} %bitcast.6, bf16[2048,768]{1,0:T(8,128)(2,1)} %bitcast.7, bf16[768,2048]{1,0:T(8,128)(2,1)} %bitcast.8), custom_call_target="tpu_custom_call" | custom-call | tf_op jit(solution)/shard_map/experts/pallas_call | solution.py:445
  69.3 1.9 %copy.9 = bf16[128,2048]{1,0:T(8,128)(2,1)} copy(bf16[128,2048]{1,0:T(8,128)(2,1)} %experts.1) | data formatting | bytes 1048576

commit v4 on v3

--- a/solution.py
+++ b/solution.py
@@ -346,13 +346,12 @@
         def add(t, h, i):
             source = order[t]
             part_copy(source, h, i).wait_recv()
-            band = pl.ds(i * step_band, step_band)
-            done[source, h, :, :, band] = (
-                part[source, h, core, :, :, band].astype(jnp.float32)
-                + part_in[source, h, :, :, band].astype(jnp.float32)
-            ).astype(jnp.bfloat16)
-            if t:
-                for j in range(i * PARTS // BANDS, (i + 1) * PARTS // BANDS):
+            for j in range(i * PARTS // BANDS, (i + 1) * PARTS // BANDS):
+                done[source, h, :, :, cols[j]] = (
+                    part[source, h, core, :, :, cols[j]].astype(jnp.float32)
+                    + part_in[source, h, :, :, cols[j]].astype(jnp.float32)
+                ).astype(jnp.bfloat16)
+                if t:
                     back_copy(source, h, j).start()
 
         def turn_over(t, h, i):

time: 71.3 us -> 71.3 us (level)
  no operation moved by 1% of the time
where the time goes in v4:
time: 71.3 us; the launch traced here: 71.1 us
  Pallas kernels  69.2 us (97%)
  local copies, waits for them, and re-layouts  1.88 us (3%)
    pallas_call x1, Pallas kernels, fused(): pl.pallas_call(kernel, out_shape=jax.ShapeDtypeStruct((tok_count, width),...  69.2 us
    unnamed x1, local copies, waits for them, and re-layouts  1.88 us

profile of v4, /device:TPU:0, one launch (start us, length us, event | category | flops | bytes accessed | tf_op | source)
XLA Modules:
  0.0 71.1 jit_solution(3702073770707420601)
XLA Ops:
  0.0 69.2 %experts.1 = bf16[128,2048]{1,0:T(8,128)(2,1)} custom-call(s32[2,128]{1,0:T(2,128)} %bitcast.10, f32[2,128]{1,0:T(2,128)} %bitcast.11, f32[1,2048]{1,0:T(1,128)} %bitcast.9, bf16[128,2048]{1,0:T(8,128)(2,1)} %tokens_hbm.1, bf16[2048,768]{1,0:T(8,128)(2,1)} %bitcast.6, bf16[2048,768]{1,0:T(8,128)(2,1)} %bitcast.7, bf16[768,2048]{1,0:T(8,128)(2,1)} %bitcast.8), custom_call_target="tpu_custom_call" | custom-call | tf_op jit(solution)/shard_map/experts/pallas_call | solution.py:444
  69.3 1.9 %copy.9 = bf16[128,2048]{1,0:T(8,128)(2,1)} copy(bf16[128,2048]{1,0:T(8,128)(2,1)} %experts.1) | data formatting | bytes 1048576
